TPU v7x, 32 devices: a whole 2x2x4 slice. The times are simulated.
32 devices in a mesh: ep: 4 (over y, x), tp: 8 (over z, core).
Axes of the slice: x: 2, y: 2, z: 4, core: 2. Of those that a mesh axis runs over, the one named last changes fastest.
Arguments:
- tokens: bfloat16 [768, 2048], P('ep'), may hold values from -6 to 6
- cotangent: bfloat16 [768, 2048], P('ep'), may hold values from -6 to 6
- routing: int32 [768, 2], P('ep'), may hold values from 0 to 3, all different within a row; in each aligned block of 192 rows (0 to 191, 192 to 383, ...) at most 192 rows name the same one
- gate_weights: bfloat16 [768, 2], P('ep'), may hold values from 0.19921875 to 1
- gate_proj: bfloat16 [4, 2048, 7168], P('ep', None, 'tp'), may hold values from -0.125 to 0.125
- up_proj: bfloat16 [4, 2048, 7168], P('ep', None, 'tp'), may hold values from -0.125 to 0.125
- down_proj: bfloat16 [4, 7168, 2048], P('ep', 'tp'), may hold values from -0.0625 to 0.0625
Outputs:
- grad_tokens: bfloat16 [768, 2048], P('ep', 'tp')
- grad_gates: float32 [768, 2], P('ep')
- grad_gate_proj: bfloat16 [4, 2048, 7168], P('ep', None, 'tp')
- grad_up_proj: bfloat16 [4, 2048, 7168], P('ep', None, 'tp')
- grad_down_proj: bfloat16 [4, 7168, 2048], P('ep', 'tp')
Inputs may be any that keep to these rules, and one draw needn't show every extreme that they name: `routing`: each row names 2 different experts. Within each aligned block of 192 rows no expert is named by more than 192 rows, and in every draw some expert is named by exactly 192 rows of some block.
All inputs are finite; a program needn't handle non-finite values.
Results may differ from a plain program's by a relative error of at most 0.019.
Values may be sent and summed in bfloat16 or wider, within the bound.
A program may use at most 128 MiB of HBM per device.

v0:
```python
import jax
import jax.numpy as jnp
from jax import lax
from jax.experimental import pallas as pl
from jax.experimental.pallas import tpu as pltpu
from jax.sharding import PartitionSpec as P


def expert_backward(in_rows, cot_rows, gate_col, w_gate, w_up, w_down):
    gate_pre = jnp.dot(in_rows, w_gate, preferred_element_type=jnp.float32)
    up_value = jnp.dot(in_rows, w_up, preferred_element_type=jnp.float32)
    sigmoid_val = jax.nn.sigmoid(gate_pre)
    active = gate_pre * sigmoid_val
    hidden = (active * up_value).astype(jnp.bfloat16)
    contract_cols = (((1,), (1,)), ((), ()))
    contract_rows = (((0,), (0,)), ((), ()))
    back_hidden = lax.dot_general(
        cot_rows, w_down, contract_cols, preferred_element_type=jnp.float32
    )
    gate_part = jnp.sum(hidden.astype(jnp.float32) * back_hidden, axis=1)
    scaled_back = gate_col * back_hidden
    grad_pre = (
        scaled_back * up_value * sigmoid_val * (1.0 + gate_pre * (1.0 - sigmoid_val))
    ).astype(jnp.bfloat16)
    grad_upval = (scaled_back * active).astype(jnp.bfloat16)
    scaled_cot = (gate_col * cot_rows.astype(jnp.float32)).astype(jnp.bfloat16)
    grad_down = lax.dot_general(
        hidden, scaled_cot, contract_rows, preferred_element_type=jnp.float32
    ).astype(jnp.bfloat16)
    grad_gate = lax.dot_general(
        in_rows, grad_pre, contract_rows, preferred_element_type=jnp.float32
    ).astype(jnp.bfloat16)
    grad_upw = lax.dot_general(
        in_rows, grad_upval, contract_rows, preferred_element_type=jnp.float32
    ).astype(jnp.bfloat16)
    grad_in = lax.dot_general(grad_pre, w_gate, contract_cols, preferred_element_type=jnp.float32)
    grad_in = grad_in + lax.dot_general(
        grad_upval, w_up, contract_cols, preferred_element_type=jnp.float32
    )
    return (grad_in, gate_part, grad_gate, grad_upw, grad_down)


def slotted(tokens, cotangent, routing, gate_weights, gate_proj, up_proj, down_proj):
    expert_count = lax.axis_size("ep")
    tok_rows, model_width = tokens.shape
    top_k = routing.shape[1]
    capacity = 2 * tok_rows * top_k // expert_count
    flat_routes = routing.reshape(-1)
    onehot = (flat_routes[:, None] == jnp.arange(expert_count, dtype=jnp.int32)[None, :]).astype(
        jnp.int32
    )
    position = jnp.sum(jnp.cumsum(onehot, axis=0) * onehot, axis=1) - 1
    slot_index = flat_routes * capacity + position
    slot_owner = (
        jnp.full((expert_count * capacity,), -1, jnp.int32)
        .at[slot_index]
        .set(jnp.arange(flat_routes.shape[0], dtype=jnp.int32))
    )
    is_used = slot_owner >= 0
    safe_owner = jnp.where(is_used, slot_owner, 0)
    token_index = safe_owner // top_k
    slot_gates = jnp.where(
        is_used, gate_weights.reshape(-1)[safe_owner], jnp.zeros((), jnp.bfloat16)
    )
    slot_gates = slot_gates.reshape(expert_count, capacity)

    def gather_slots(source):
        picked_rows = jnp.where(is_used[:, None], source[token_index], jnp.zeros((), jnp.bfloat16))
        return picked_rows.reshape(expert_count, capacity, source.shape[1])

    col_width = model_width // lax.axis_size("tp")
    col_start = lax.axis_index("tp") * col_width
    token_cols = lax.dynamic_slice_in_dim(tokens, col_start, col_width, 1)
    cot_cols = lax.dynamic_slice_in_dim(cotangent, col_start, col_width, 1)
    rows_part, cots_part, gates_in = (
        lax.all_to_all(gather_slots(token_cols), "ep", split_axis=0, concat_axis=0, tiled=True),
        lax.all_to_all(gather_slots(cot_cols), "ep", split_axis=0, concat_axis=0, tiled=True),
        lax.all_to_all(slot_gates, "ep", split_axis=0, concat_axis=0, tiled=True),
    )
    in_rows, cot_in = (
        lax.all_gather(rows_part, "tp", axis=2, tiled=True),
        lax.all_gather(cots_part, "tp", axis=2, tiled=True),
    )
    slot_count = in_rows.shape[0] * in_rows.shape[1]
    grad_in, gate_part, grad_gate, grad_upw, grad_down = expert_backward(
        in_rows.reshape(slot_count, model_width),
        cot_in.reshape(slot_count, model_width),
        gates_in.reshape(slot_count, 1).astype(jnp.float32),
        gate_proj[0],
        up_proj[0],
        down_proj[0],
    )
    gate_total = lax.psum(gate_part, "tp")
    grad_cols = lax.psum_scatter(
        grad_in.astype(jnp.bfloat16), "tp", scatter_dimension=1, tiled=True
    ).astype(jnp.float32)
    back_rows, back_gates = (
        lax.all_to_all(
            grad_cols.reshape(expert_count, capacity, grad_cols.shape[1]).astype(jnp.bfloat16),
            "ep",
            split_axis=0,
            concat_axis=0,
            tiled=True,
        ).astype(jnp.float32),
        lax.all_to_all(
            gate_total.reshape(expert_count, capacity).astype(jnp.bfloat16),
            "ep",
            split_axis=0,
            concat_axis=0,
            tiled=True,
        ).astype(jnp.float32),
    )
    picked = back_rows.reshape(expert_count * capacity, back_rows.shape[2])[slot_index]
    grad_tokens = jnp.sum(picked.reshape(tok_rows, top_k, picked.shape[1]), axis=1).astype(
        jnp.bfloat16
    )
    grad_gates = back_gates.reshape(-1)[slot_index].reshape(tok_rows, top_k)
    return (grad_tokens, grad_gates, grad_gate[None], grad_upw[None], grad_down[None])


MESH = pl.DeviceIdType.MESH


def flip(index, mask):
    if mask & 1:
        index = index + 1 - 2 * (index % 2)
    if mask & 2:
        index = index + 2 - 4 * ((index // 2) % 2)
    if mask & 4:
        index = index + 4 - 8 * ((index // 4) % 2)
    return index


class Copies:
    def __init__(self, send_sem, recv_sem):
        self.send_sem, self.recv_sem, self.made = send_sem, recv_sem, []

    def send(self, src, dst, ep, tp):
        n = len(self.made)
        copy = pltpu.make_async_remote_copy(
            src_ref=src,
            dst_ref=dst,
            send_sem=self.send_sem.at[n],
            recv_sem=self.recv_sem.at[n],
            device_id=(ep, tp),
            device_id_type=MESH,
        )
        copy.start()
        self.made.append(copy)
        return copy

    def finish(self):
        for copy in self.made:
            copy.wait_send()


def gather_kernel(tok, cot, gate, tok_out, cot_out, gate_out, send_sem, recv_sem, own_sem):
    me, t = lax.axis_index("ep"), lax.axis_index("tp")
    width = tok.shape[1]
    eighth = width // 8
    quarter = 2 * eighth
    q, far = t % 4, flip(t % 4, 2)

    def cols(start, size):
        return pl.ds(pl.multiple_of(start, 128), size)

    low, high = cols(quarter * q, eighth), cols(quarter * q + eighth, eighth)
    full = cols(quarter * q, quarter)
    far_low, far_high = cols(quarter * far, eighth), cols(quarter * far + eighth, eighth)
    far_full = cols(quarter * far, quarter)
    pairs = ((tok, tok_out), (cot, cot_out))
    own = [
        pltpu.make_async_copy(src, dst.at[0], own_sem.at[a]) for a, (src, dst) in enumerate(pairs)
    ]
    for copy in own:
        copy.start()
    do = Copies(send_sem, recv_sem)
    gates = [do.send(gate.at[j], gate_out.at[j], flip(me, j), t) for j in (1, 2, 3)]
    relayed, direct = [], []
    for src, dst in pairs:
        for j, where in ((3, full), (1, high), (2, high)):
            copy = do.send(src.at[:, where], dst.at[j, :, where], flip(me, j), t)
            relayed.append((copy, dst, j, where))
    for src, dst in pairs:
        for where in (low, far_low):
            for j in (1, 2):
                copy = do.send(src.at[:, where], dst.at[j, :, where], flip(me, j), t)
                direct.append((copy, dst, j, where))
    last = []
    for copy, dst, j, where in relayed:
        copy.wait_recv()
        piece = dst.at[j, :, where]
        moved = do.send(piece, piece, me, flip(t, 2))
        direct.append((moved, dst, j, far_full if j == 3 else far_high))
        last.append(do.send(piece, piece, me, flip(t, 1)))
    for copy, dst, j, where in direct:
        copy.wait_recv()
        piece = dst.at[j, :, where]
        last.append(do.send(piece, piece, me, flip(t, 1)))
    for copy in last + gates:
        copy.wait_recv()
    do.finish()
    gate_out[0] = gate[0]
    for copy in own:
        copy.wait()


def gather(tokens, cotangent, gate):
    experts = lax.axis_size("ep")
    shape = jax.ShapeDtypeStruct((experts,) + tokens.shape, tokens.dtype)
    vmem = pl.BlockSpec(memory_space=pltpu.VMEM)
    return pl.pallas_call(
        gather_kernel,
        out_shape=[shape, shape, jax.ShapeDtypeStruct(gate.shape, gate.dtype)],
        in_specs=[vmem] * 3,
        out_specs=[vmem] * 3,
        scratch_shapes=[
            pltpu.SemaphoreType.DMA((43,)),
            pltpu.SemaphoreType.DMA((43,)),
            pltpu.SemaphoreType.DMA((2,)),
        ],
        compiler_params=pltpu.CompilerParams(has_side_effects=True, vmem_limit_bytes=14 << 20),
    )(tokens, cotangent, gate)


def reduce_kernel(part, gate, out, gate_out, r1, m, r2, s, r3, rg, g, send_sem, recv_sem):
    me, t = lax.axis_index("ep"), lax.axis_index("tp")
    core, z = t % 2, t // 2
    size = out.shape[1]
    other = flip(t, 1)
    order = (3, 2, 1, 0)
    blocks = (3, 1, 2, 0)
    f32 = jnp.float32

    def cols(d, which):
        return pl.ds(pl.multiple_of((2 * flip(z, d) + which) * size, 128), size)

    do = Copies(send_sem, recv_sem)
    first = {}
    for d in order:
        for j in blocks:
            first[d, j] = do.send(part.at[j, :, cols(d, 1 - core)], r1.at[d, j], me, other)
        if d == 3:
            stage = do.send(gate, rg.at[0], me, other)
    second = {}
    for n, d in enumerate(order):
        for j in blocks:
            first[d, j].wait_recv()
            mine = part[j, :, cols(d, core)].astype(f32)
            m[d, j] = (mine + r1[d, j].astype(f32)).astype(m.dtype)
            if j > 0:
                second[d, j] = do.send(m.at[d, j], r2.at[d, j], flip(me, j), t)
        if n < 3:
            stage.wait_recv()
            g[n] = (gate[...] if n == 0 else g[n - 1]) + rg[n]
            if n < 2:
                stage = do.send(g.at[n], rg.at[n + 1], me, flip(t, 2 << n))
    gates = [do.send(g.at[2, j], gate_out.at[j], flip(me, j), t) for j in (1, 2, 3)]
    third = {}
    for d in order:
        total = m[d, 0].astype(f32)
        for j in (1, 2, 3):
            second[d, j].wait_recv()
            total = total + r2[d, j].astype(f32)
        if d:
            s[d] = total.astype(s.dtype)
            third[d] = do.send(s.at[d], r3.at[d], me, flip(t, 2 * d))
    for d in (3, 2, 1):
        third[d].wait_recv()
        total = total + r3[d].astype(f32)
    out[...] = total.astype(out.dtype)
    for copy in gates:
        copy.wait_recv()
    do.finish()
    gate_out[0] = g[2, 0]


def reduce(part, gate):
    experts, parts = lax.axis_size("ep"), lax.axis_size("tp")
    rows, size = part.shape[1], part.shape[2] // parts
    vmem = pl.BlockSpec(memory_space=pltpu.VMEM)
    slots = parts // 2
    tile = pltpu.VMEM((slots, experts, rows, size), part.dtype)
    return pl.pallas_call(
        reduce_kernel,
        out_shape=[
            jax.ShapeDtypeStruct((rows, size), part.dtype),
            jax.ShapeDtypeStruct(gate.shape, gate.dtype),
        ],
        in_specs=[vmem] * 2,
        out_specs=[vmem] * 2,
        scratch_shapes=[
            tile,
            tile,
            tile,
            pltpu.VMEM((slots, rows, size), part.dtype),
            pltpu.VMEM((slots, rows, size), part.dtype),
            pltpu.VMEM((3,) + gate.shape, gate.dtype),
            pltpu.VMEM((3,) + gate.shape, gate.dtype),
            pltpu.SemaphoreType.DMA((37,)),
            pltpu.SemaphoreType.DMA((37,)),
        ],
        compiler_params=pltpu.CompilerParams(has_side_effects=True, vmem_limit_bytes=20 << 20),
    )(part, gate)


def tiles(values):
    rows = values.shape[1]
    padded = jnp.pad(values, ((0, 0), (0, -rows % 128)))
    return jnp.broadcast_to(padded[:, None, :], (padded.shape[0], 8, padded.shape[1]))


def dense(tokens, cotangent, routing, gate_weights, gate_proj, up_proj, down_proj):
    f32, bf16 = jnp.float32, jnp.bfloat16
    experts = lax.axis_size("ep")
    rows, width = tokens.shape
    me = lax.axis_index("ep")
    named = [routing == (me ^ j) for j in range(experts)]
    weights = jnp.stack(
        [jnp.sum(jnp.where(n, gate_weights.astype(f32), 0.0), axis=1) for n in named]
    )
    x_all, cot_all, g_all = gather(tokens, cotangent, tiles(weights))
    x, cot = x_all.reshape(-1, width), cot_all.reshape(-1, width)
    g = g_all[:, 0, :rows].reshape(-1, 1)
    grad_in, gate_part, d_gate, d_up, d_down = expert_backward(
        x, cot, g, gate_proj[0], up_proj[0], down_proj[0]
    )
    grad_tokens, gate_sum = reduce(
        grad_in.astype(bf16).reshape(experts, rows, width),
        tiles(gate_part.reshape(experts, rows)),
    )
    grad_gates = jnp.zeros(routing.shape, f32)
    for j in range(experts):
        grad_gates = jnp.where(named[j], gate_sum[j, 0, :rows][:, None], grad_gates)
    return grad_tokens, grad_gates, d_gate[None], d_up[None], d_down[None]


def local(tokens, cotangent, routing, gate_weights, gate_proj, up_proj, down_proj):
    experts, parts = lax.axis_size("ep"), lax.axis_size("tp")
    capacity = 2 * tokens.shape[0] * routing.shape[1] // experts
    fits = experts == 4 and parts == 8 and tokens.shape[1] % 1024 == 0
    plan = dense if capacity >= tokens.shape[0] and fits else slotted
    return plan(tokens, cotangent, routing, gate_weights, gate_proj, up_proj, down_proj)


def solution(mesh):
    return jax.shard_map(
        local,
        mesh=mesh,
        in_specs=(
            P("ep", None),
            P("ep", None),
            P("ep", None),
            P("ep", None),
            P("ep", None, "tp"),
            P("ep", None, "tp"),
            P("ep", "tp", None),
        ),
        out_specs=(
            P("ep", "tp"),
            P("ep", None),
            P("ep", None, "tp"),
            P("ep", None, "tp"),
            P("ep", "tp", None),
        ),
        check_vma=False,
    )
```

profile of v0, /device:TPU:0, one launch (start us, length us, event | category | flops | bytes accessed | tf_op | source)
XLA Modules:
  0.0 113.3 jit_solution(5648277116402617579)
XLA Ops:
  0.6 0.7 fusion.14
  1.4 0.0 copy-start
  1.4 1.1 copy-done
  2.5 0.0 copy-start.1
  2.5 1.1 copy-done.1
  3.7 36.0 %shard_map.110 = (bf16[4,192,2048]{2,1,0:T(8,128)(2,1)S(1)}, bf16[4,192,2048]{2,1,0:T(8,128)(2,1)S(1)}, f32[4,8,256]{2,1,0:T(8,128)S(1)}) custom-call(bf16[192,2048]{1,0:T(8,128)(2,1)S(1)} %copy-done, bf16[192,2048]{1,0:T(8,128)(2,1)S(1)} %copy-done.1, f32[4,8,256]{2,1,0:T(8,128)S(1)} %broadcast_in_dim.61.gate), custom_call_target="tpu_custom_call" | custom-call | tf_op jit(solution)/shard_map/pallas_call | solution.py:212
  39.6 0.0 copy-start.4
  39.7 0.0 copy-start.2
  39.7 0.0 copy-start.7
  39.7 9.3 %fusion.6 = f32[768,896]{1,0:T(8,128)} fusion(bf16[768,2048]{1,0:T(8,128)(2,1)S(1)} %bitcast.47, bf16[1,2048,896]{2,1,0:T(8,128)(2,1)} %param.12), kind=kOutput, calls=%fused_computation.8 | convolution fusion | flops 2818572288 | bytes 9568256 | tf_op jit(solution)/shard_map/dot_general | solution.py:11
  49.0 0.0 copy-done.4
  49.0 0.0 copy-done.7
  49.0 4.9 %fusion.2 = f32[768,896]{1,0:T(8,128)} fusion(bf16[768,2048]{1,0:T(8,128)(2,1)S(1)} %bitcast.48, bf16[1,2048,896]{2,1,0:T(8,128)(2,1)S(1)} %copy-done.7), kind=kOutput, calls=%fused_computation.4 | convolution fusion | flops 2818572288 | bytes 9568256 | tf_op jit(solution)/shard_map/dot_general | solution.py:10
  53.9 0.1 mul.42
  54.0 0.0 copy-done.2
  54.0 0.0 copy-start.8
  54.0 8.6 %multiply_reduce_fusion = (f32[768]{0:T(1024)S(1)}, bf16[768,896]{1,0:T(8,128)(2,1)}, bf16[768,896]{1,0:T(8,128)(2,1)S(1)}, bf16[768,896]{1,0:T(8,128)(2,1)S(1)}) fusion(f32[768,896]{1,0:T(8,128)} %fusion.6, f32[768,896]{1,0:T(8,128)} %fusion.2, f32[768]{0:T(1024)S(1)} %mul.42, bf16[768,2048]{1,0:T(8,128)(2,1)S(1)} %bitcast.45, bf16[1,896,2048]{2,1,0:T(8,128)(2,1)} %param.13), kind=kOutput, calls=%fused_computation.16 | convolution fusion | flops 2831645952 | bytes 16455680 | tf_op jit(solution)/shard_map/dot_general | solution.py:17
  62.6 0.0 copy-start.11
  62.6 0.0 copy-start.10
  62.6 0.0 copy-done.8
  62.6 0.0 copy-start.9
  62.6 3.4 %fusion = f32[768,2048]{1,0:T(8,128)S(1)} fusion(bf16[768,896]{1,0:T(8,128)(2,1)S(1)} %get-tuple-element.21, bf16[1,2048,896]{2,1,0:T(8,128)(2,1)S(1)} %copy-done.8), kind=kOutput, calls=%fused_computation.2 | convolution fusion | flops 2818572288 | bytes 11337728 | tf_op jit(solution)/shard_map/dot_general | solution.py:36
  66.1 0.0 copy-done.11
  66.1 0.0 copy-done.9
  66.1 3.7 %add_convert_fusion = bf16[768,2048]{1,0:T(8,128)(2,1)S(1)} fusion(f32[768,2048]{1,0:T(8,128)S(1)} %fusion, bf16[768,896]{1,0:T(8,128)(2,1)S(1)} %get-tuple-element.22, bf16[1,2048,896]{2,1,0:T(8,128)(2,1)S(1)} %copy-done.9), kind=kOutput, calls=%fused_computation.1 | convolution fusion | flops 2821718016 | bytes 14483456 | tf_op jit(solution)/shard_map/dot_general | solution.py:37
  69.8 0.0 copy-done.10
  69.8 0.0 copy-start.6
  69.8 0.1 reshape.32
  69.9 0.0 copy-start.5
  69.9 26.1 %shard_map.111 = (bf16[192,256]{1,0:T(8,128)(2,1)S(1)}, f32[4,8,256]{2,1,0:T(8,128)S(1)}) custom-call(bf16[4,192,2048]{2,1,0:T(8,128)(2,1)S(1)} %bitcast.44, f32[4,8,256]{2,1,0:T(8,128)S(1)} %broadcast_in_dim.62.gate), custom_call_target="tpu_custom_call" | custom-call | tf_op jit(solution)/shard_map/pallas_call | solution.py:284
  96.0 0.0 copy-done.6
  96.0 0.6 select_select_fusion
  96.6 0.0 copy-done.5
  96.6 0.0 copy-start.12
  96.6 6.4 %convert_bitcast_fusion.2 = bf16[1,2048,896]{2,1,0:T(8,128)(2,1)} fusion(bf16[768,2048]{1,0:T(8,128)(2,1)S(1)} %bitcast.49, bf16[768,896]{1,0:T(8,128)(2,1)} %copy-done.10), kind=kOutput, calls=%fused_computation.14 | convolution fusion | flops 2820407296 | bytes 8192000 | tf_op jit(solution)/shard_map/dot_general | solution.py:30
  103.0 0.0 copy-done.12
  103.0 0.0 copy-start.3
  103.0 0.0 copy-start.13
  103.0 5.0 %convert_bitcast_fusion.1 = bf16[1,2048,896]{2,1,0:T(8,128)(2,1)} fusion(bf16[768,2048]{1,0:T(8,128)(2,1)S(1)} %bitcast.50, bf16[768,896]{1,0:T(8,128)(2,1)S(1)} %copy-done.12), kind=kOutput, calls=%fused_computation.13 | convolution fusion | flops 2820407296 | bytes 8192000 | tf_op jit(solution)/shard_map/dot_general | solution.py:33
  108.0 0.0 copy-done.3
  108.0 0.0 copy-done.13
  108.0 4.7 %convert_bitcast_fusion = bf16[1,896,2048]{2,1,0:T(8,128)(2,1)} fusion(bf16[768,896]{1,0:T(8,128)(2,1)S(1)} %copy-done.13, bf16[768,2048]{1,0:T(8,128)(2,1)S(1)} %bitcast.46, f32[768]{0:T(1024)S(1)} %mul.42), kind=kOutput, calls=%fused_computation.12 | convolution fusion | flops 2825125888 | bytes 8195072 | tf_op jit(solution)/shard_map/dot_general | solution.py:27
  112.6 0.6 copy.13
  (6 shorter events, 0.1 us)
Async XLA Ops:
  1.4 1.1 %copy-start = (bf16[192,2048]{1,0:T(8,128)(2,1)S(1)}, bf16[192,2048]{1,0:T(8,128)(2,1)}, u32[]{:S(2)}) copy-start(bf16[192,2048]{1,0:T(8,128)(2,1)} %tok.1) | copy-start | bytes 2359300
  2.5 1.1 %copy-start.1 = (bf16[192,2048]{1,0:T(8,128)(2,1)S(1)}, bf16[192,2048]{1,0:T(8,128)(2,1)}, u32[]{:S(2)}) copy-start(bf16[192,2048]{1,0:T(8,128)(2,1)} %cot.1) | copy-start | bytes 2359300
  39.6 9.3 %copy-start.4 = (bf16[4,192,2048]{2,1,0:T(8,128)(2,1)}, bf16[4,192,2048]{2,1,0:T(8,128)(2,1)S(1)}, u32[]{:S(2)}) copy-start(bf16[4,192,2048]{2,1,0:T(8,128)(2,1)S(1)} %get-tuple-element.12) | copy-start | bytes 9437188
  39.7 14.4 %copy-start.2 = (bf16[4,192,2048]{2,1,0:T(8,128)(2,1)}, bf16[4,192,2048]{2,1,0:T(8,128)(2,1)S(1)}, u32[]{:S(2)}) copy-start(bf16[4,192,2048]{2,1,0:T(8,128)(2,1)S(1)} %get-tuple-element.11) | copy-start | bytes 9437188
  39.7 9.3 %copy-start.7 = (bf16[1,2048,896]{2,1,0:T(8,128)(2,1)S(1)}, bf16[1,2048,896]{2,1,0:T(8,128)(2,1)}, u32[]{:S(2)}) copy-start(bf16[1,2048,896]{2,1,0:T(8,128)(2,1)} %param.11) | copy-start | bytes 11010052
  54.0 8.6 %copy-start.8 = (bf16[1,2048,896]{2,1,0:T(8,128)(2,1)S(1)}, bf16[1,2048,896]{2,1,0:T(8,128)(2,1)}, u32[]{:S(2)}) copy-start(bf16[1,2048,896]{2,1,0:T(8,128)(2,1)} %param.11) | copy-start | bytes 11010052
  62.6 3.5 %copy-start.11 = (bf16[768,896]{1,0:T(8,128)(2,1)}, bf16[768,896]{1,0:T(8,128)(2,1)S(1)}, u32[]{:S(2)}) copy-start(bf16[768,896]{1,0:T(8,128)(2,1)S(1)} %get-tuple-element.22) | copy-start | bytes 4128772
  62.6 7.2 %copy-start.10 = (bf16[768,896]{1,0:T(8,128)(2,1)}, bf16[768,896]{1,0:T(8,128)(2,1)S(1)}, u32[]{:S(2)}) copy-start(bf16[768,896]{1,0:T(8,128)(2,1)S(1)} %get-tuple-element.21) | copy-start | bytes 4128772
  62.6 3.5 %copy-start.9 = (bf16[1,2048,896]{2,1,0:T(8,128)(2,1)S(1)}, bf16[1,2048,896]{2,1,0:T(8,128)(2,1)}, u32[]{:S(2)}) copy-start(bf16[1,2048,896]{2,1,0:T(8,128)(2,1)} %param.12) | copy-start | bytes 11010052
  69.8 26.2 %copy-start.6 = (s32[192,2]{0,1:T(2,128)S(1)}, s32[192,2]{0,1:T(2,128)}, u32[]{:S(2)}) copy-start(s32[192,2]{0,1:T(2,128)} %param.9) | copy-start | bytes 4612
  69.9 26.7 %copy-start.5 = (bf16[4,192,2048]{2,1,0:T(8,128)(2,1)S(1)}, bf16[4,192,2048]{2,1,0:T(8,128)(2,1)}, u32[]{:S(2)}) copy-start(bf16[4,192,2048]{2,1,0:T(8,128)(2,1)} %copy-done.4) | copy-start | bytes 9437188
  96.6 6.4 %copy-start.12 = (bf16[768,896]{1,0:T(8,128)(2,1)S(1)}, bf16[768,896]{1,0:T(8,128)(2,1)}, u32[]{:S(2)}) copy-start(bf16[768,896]{1,0:T(8,128)(2,1)} %copy-done.11) | copy-start | bytes 4128772
  103.0 5.0 %copy-start.3 = (bf16[4,192,2048]{2,1,0:T(8,128)(2,1)S(1)}, bf16[4,192,2048]{2,1,0:T(8,128)(2,1)}, u32[]{:S(2)}) copy-start(bf16[4,192,2048]{2,1,0:T(8,128)(2,1)} %copy-done.2) | copy-start | bytes 9437188
  103.0 5.0 %copy-start.13 = (bf16[768,896]{1,0:T(8,128)(2,1)S(1)}, bf16[768,896]{1,0:T(8,128)(2,1)}, u32[]{:S(2)}) copy-start(bf16[768,896]{1,0:T(8,128)(2,1)} %get-tuple-element.20) | copy-start | bytes 4128772
where the time goes:
time: 114 us; the launch traced here: 113 us
  Pallas kernels  62.1 us (54%)
  matrix products  45.9 us (40%)
  local copies, waits for them, and re-layouts  3.16 us (3%)
  other arithmetic  1.33 us (1%)
    pallas_call x1, Pallas kernels, gather(): pl.pallas_call(gather_kernel, out_shape=[shape, shape, jax.ShapeDtypeStru...  36 us
    pallas_call x1, Pallas kernels, reduce(): pl.pallas_call(reduce_kernel, out_shape=[jax.ShapeDtypeStruct((rows, size...  26.1 us
    dot_general x1, matrix products, expert_backward(): up_value = jnp.dot(in_rows, w_up, preferred_element_type=jnp.float32)  9.28 us
    dot_general x1, matrix products, expert_backward(): lax.dot_general(cot_rows, w_down, contract_cols, preferred_element_type=j...  8.58 us
    dot_general x1, matrix products, expert_backward(): lax.dot_general(in_rows, grad_pre, contract_rows, preferred_element_type=...  6.36 us
    dot_general x1, matrix products, expert_backward(): lax.dot_general(in_rows, grad_upval, contract_rows, preferred_element_typ...  4.97 us
    dot_general x1, matrix products, expert_backward(): gate_pre = jnp.dot(in_rows, w_gate, preferred_element_type=jnp.float32)  4.94 us
    dot_general x1, matrix products, expert_backward(): lax.dot_general(hidden, scaled_cot, contract_rows, preferred_element_type...  4.66 us

commit v1 on v0

v1 whole, which is shorter than its diff:
```python
import jax
import jax.numpy as jnp
from jax import lax
from jax.experimental import pallas as pl
from jax.experimental.pallas import tpu as pltpu
from jax.sharding import PartitionSpec as P


def expert_backward(in_rows, cot_rows, gate_col, w_gate, w_up, w_down):
    gate_pre = jnp.dot(in_rows, w_gate, preferred_element_type=jnp.float32)
    up_value = jnp.dot(in_rows, w_up, preferred_element_type=jnp.float32)
    sigmoid_val = jax.nn.sigmoid(gate_pre)
    active = gate_pre * sigmoid_val
    hidden = (active * up_value).astype(jnp.bfloat16)
    contract_cols = (((1,), (1,)), ((), ()))
    contract_rows = (((0,), (0,)), ((), ()))
    back_hidden = lax.dot_general(
        cot_rows, w_down, contract_cols, preferred_element_type=jnp.float32
    )
    gate_part = jnp.sum(hidden.astype(jnp.float32) * back_hidden, axis=1)
    scaled_back = gate_col * back_hidden
    grad_pre = (
        scaled_back * up_value * sigmoid_val * (1.0 + gate_pre * (1.0 - sigmoid_val))
    ).astype(jnp.bfloat16)
    grad_upval = (scaled_back * active).astype(jnp.bfloat16)
    scaled_cot = (gate_col * cot_rows.astype(jnp.float32)).astype(jnp.bfloat16)
    grad_down = lax.dot_general(
        hidden, scaled_cot, contract_rows, preferred_element_type=jnp.float32
    ).astype(jnp.bfloat16)
    grad_gate = lax.dot_general(
        in_rows, grad_pre, contract_rows, preferred_element_type=jnp.float32
    ).astype(jnp.bfloat16)
    grad_upw = lax.dot_general(
        in_rows, grad_upval, contract_rows, preferred_element_type=jnp.float32
    ).astype(jnp.bfloat16)
    grad_in = lax.dot_general(grad_pre, w_gate, contract_cols, preferred_element_type=jnp.float32)
    grad_in = grad_in + lax.dot_general(
        grad_upval, w_up, contract_cols, preferred_element_type=jnp.float32
    )
    return (grad_in, gate_part, grad_gate, grad_upw, grad_down)


def slotted(tokens, cotangent, routing, gate_weights, gate_proj, up_proj, down_proj):
    expert_count = lax.axis_size("ep")
    tok_rows, model_width = tokens.shape
    top_k = routing.shape[1]
    capacity = 2 * tok_rows * top_k // expert_count
    flat_routes = routing.reshape(-1)
    onehot = (flat_routes[:, None] == jnp.arange(expert_count, dtype=jnp.int32)[None, :]).astype(
        jnp.int32
    )
    position = jnp.sum(jnp.cumsum(onehot, axis=0) * onehot, axis=1) - 1
    slot_index = flat_routes * capacity + position
    slot_owner = (
        jnp.full((expert_count * capacity,), -1, jnp.int32)
        .at[slot_index]
        .set(jnp.arange(flat_routes.shape[0], dtype=jnp.int32))
    )
    is_used = slot_owner >= 0
    safe_owner = jnp.where(is_used, slot_owner, 0)
    token_index = safe_owner // top_k
    slot_gates = jnp.where(
        is_used, gate_weights.reshape(-1)[safe_owner], jnp.zeros((), jnp.bfloat16)
    )
    slot_gates = slot_gates.reshape(expert_count, capacity)

    def gather_slots(source):
        picked_rows = jnp.where(is_used[:, None], source[token_index], jnp.zeros((), jnp.bfloat16))
        return picked_rows.reshape(expert_count, capacity, source.shape[1])

    col_width = model_width // lax.axis_size("tp")
    col_start = lax.axis_index("tp") * col_width
    token_cols = lax.dynamic_slice_in_dim(tokens, col_start, col_width, 1)
    cot_cols = lax.dynamic_slice_in_dim(cotangent, col_start, col_width, 1)
    rows_part, cots_part, gates_in = (
        lax.all_to_all(gather_slots(token_cols), "ep", split_axis=0, concat_axis=0, tiled=True),
        lax.all_to_all(gather_slots(cot_cols), "ep", split_axis=0, concat_axis=0, tiled=True),
        lax.all_to_all(slot_gates, "ep", split_axis=0, concat_axis=0, tiled=True),
    )
    in_rows, cot_in = (
        lax.all_gather(rows_part, "tp", axis=2, tiled=True),
        lax.all_gather(cots_part, "tp", axis=2, tiled=True),
    )
    slot_count = in_rows.shape[0] * in_rows.shape[1]
    grad_in, gate_part, grad_gate, grad_upw, grad_down = expert_backward(
        in_rows.reshape(slot_count, model_width),
        cot_in.reshape(slot_count, model_width),
        gates_in.reshape(slot_count, 1).astype(jnp.float32),
        gate_proj[0],
        up_proj[0],
        down_proj[0],
    )
    gate_total = lax.psum(gate_part, "tp")
    grad_cols = lax.psum_scatter(
        grad_in.astype(jnp.bfloat16), "tp", scatter_dimension=1, tiled=True
    ).astype(jnp.float32)
    back_rows, back_gates = (
        lax.all_to_all(
            grad_cols.reshape(expert_count, capacity, grad_cols.shape[1]).astype(jnp.bfloat16),
            "ep",
            split_axis=0,
            concat_axis=0,
            tiled=True,
        ).astype(jnp.float32),
        lax.all_to_all(
            gate_total.reshape(expert_count, capacity).astype(jnp.bfloat16),
            "ep",
            split_axis=0,
            concat_axis=0,
            tiled=True,
        ).astype(jnp.float32),
    )
    picked = back_rows.reshape(expert_count * capacity, back_rows.shape[2])[slot_index]
    grad_tokens = jnp.sum(picked.reshape(tok_rows, top_k, picked.shape[1]), axis=1).astype(
        jnp.bfloat16
    )
    grad_gates = back_gates.reshape(-1)[slot_index].reshape(tok_rows, top_k)
    return (grad_tokens, grad_gates, grad_gate[None], grad_upw[None], grad_down[None])


MESH = pl.DeviceIdType.MESH
F32, BF16 = jnp.float32, jnp.bfloat16
NT = (((1,), (1,)), ((), ()))
TN = (((0,), (0,)), ((), ()))


def flip(index, mask):
    if mask & 1:
        index = index + 1 - 2 * (index % 2)
    if mask & 2:
        index = index + 2 - 4 * ((index // 2) % 2)
    if mask & 4:
        index = index + 4 - 8 * ((index // 4) % 2)
    return index


def lanes(start, size, unit=128):
    return pl.ds(pl.multiple_of(start, unit), size)


class Copies:
    def __init__(self, send_sem, recv_sem):
        self.send_sem, self.recv_sem, self.made = send_sem, recv_sem, []

    def send(self, src, dst, ep, tp):
        n = len(self.made)
        copy = pltpu.make_async_remote_copy(
            src_ref=src,
            dst_ref=dst,
            send_sem=self.send_sem.at[n],
            recv_sem=self.recv_sem.at[n],
            device_id=(ep, tp),
            device_id_type=MESH,
        )
        copy.start()
        self.made.append(copy)
        return copy

    def finish(self):
        for copy in self.made:
            copy.wait_send()


def layer_kernel(
    tok, cot, routing, gates, w_gate, w_up, w_down,
    out, gates_out, d_gate, d_up, d_down,
    x, c, scaled, wcat, wd, pu, hcat, hid, part,
    gs, gin, gcol, gacc, r1, m, r2, s, r3, gp, rg, gt, go,
    send_sem, recv_sem, own_sem,
):
    me, t = lax.axis_index("ep"), lax.axis_index("tp")
    core, z = t % 2, t // 2
    rows, width = tok.shape
    units = w_gate.shape[1]
    full_tiles = units // 256
    size = out.shape[1]
    eighth = width // 8
    quarter = 2 * eighth
    chunk = 2 * size
    q, far = t % 4, flip(t % 4, 2)
    other = flip(t, 1)
    blocks = {j: pl.ds(j * rows, rows) for j in range(4)}

    n = 0
    loads = []
    for src, dst in ((tok, x), (cot, c)):
        loads.append(pltpu.make_async_copy(src, dst.at[blocks[0]], own_sem.at[n]))
        n += 1
    weights = []
    for k in range(units // 128):
        for a, w in enumerate((w_gate, w_up)):
            weights.append(
                pltpu.make_async_copy(
                    w.at[:, pl.ds(128 * k, 128)],
                    wcat.at[:, pl.ds(256 * k + 128 * a, 128)],
                    own_sem.at[n],
                )
            )
            n += 1
    weights.append(pltpu.make_async_copy(w_down, wd, own_sem.at[n]))
    for copy in loads + weights:
        copy.start()

    barrier = pltpu.get_barrier_semaphore()
    partners = [(flip(me, j), t) for j in (1, 2, 3)] + [(me, flip(t, k)) for k in (1, 2, 4, 6)]
    for device in partners:
        pl.semaphore_signal(barrier, inc=1, device_id=device, device_id_type=MESH)

    gs[...] = jnp.zeros_like(gs)
    gacc[...] = jnp.zeros_like(gacc)
    routes, weight = routing[...], gates[...].astype(F32)
    for j in range(4):
        row = jnp.sum(jnp.where(routes == flip(me, j), weight, 0.0), axis=0, keepdims=True)
        gs[j, :, 0:rows] = jnp.broadcast_to(row, (8, rows))
    pl.semaphore_wait(barrier, len(partners))

    do = Copies(send_sem, recv_sem)
    for copy in loads:
        copy.wait()
    gate_in = [do.send(gs.at[j], gin.at[j], flip(me, j), t) for j in (1, 2, 3)]

    def ep_send(a, j, cols):
        ref = both[a]
        copy = do.send(ref.at[blocks[0], cols], ref.at[blocks[j], cols], flip(me, j), t)
        return (copy, a, j, cols)

    def relay(item, mask):
        piece = both[item[1]].at[blocks[item[2]], item[3]]
        return do.send(piece, piece, me, flip(t, mask))

    low, high = lanes(quarter * q, eighth), lanes(quarter * q + eighth, eighth)
    far_low, far_high = lanes(quarter * far, eighth), lanes(quarter * far + eighth, eighth)
    both = (x, c)
    near, direct = {}, {}
    for ref in (0, 1):
        near[ref] = [ep_send(ref, 1, high), ep_send(ref, 2, high)]
        near[ref] += [ep_send(ref, 3, low), ep_send(ref, 3, high)]
    for ref in (0, 1):
        direct[ref] = [ep_send(ref, j, w) for w in (low, far_low) for j in (1, 2)]
    mirror = [far_high, far_high, far_low, far_high]
    moved = ([], [])
    landed = ([], [])

    def pass_near(ref, part_of):
        for n in part_of:
            item = near[ref][n]
            item[0].wait_recv()
            moved[ref].append((relay(item, 2), ref, item[2], mirror[n]))
            landed[ref].append(relay(item, 1))

    def pass_on(items):
        for item in items:
            item[0].wait_recv()
            landed[item[1]].append(relay(item, 1))

    def gate_up(at, count):
        def tile(start, size_of):
            cols = lanes(start, size_of, 256)
            pu[at, cols] = jnp.dot(x[at, :], wcat[:, cols], preferred_element_type=F32)

        def body(k, carry):
            tile(512 * k, 512)
            return carry

        lax.fori_loop(0, full_tiles, body, 0)
        if units % 256:
            tile(512 * full_tiles, 256)

    def back_of(at, js):
        def tile(start, size_of):
            unit = lanes(start, size_of)
            back_all = lax.dot_general(c[at, :], wd[unit, :], NT, preferred_element_type=F32)
            for n, j in enumerate(js):
                mine = slice(n * rows, (n + 1) * rows)
                g = gcol[j]
                total = gacc[j, 0:rows, :]
                for k in range(size_of // 128):
                    pre = pu[blocks[j], lanes(2 * start + 256 * k, 128)]
                    up = pu[blocks[j], lanes(2 * start + 256 * k + 128, 128)]
                    back = back_all[mine, 128 * k : 128 * k + 128]
                    sig = jax.nn.sigmoid(pre)
                    act = pre * sig
                    hidden = (act * up).astype(BF16)
                    total = total + hidden.astype(F32) * back
                    scaled_back = g * back
                    grad_pre = scaled_back * up * sig * (1.0 + pre * (1.0 - sig))
                    hid[blocks[j], lanes(start + 128 * k, 128)] = hidden
                    hcat[blocks[j], lanes(2 * start + 256 * k, 128)] = grad_pre.astype(BF16)
                    hcat[blocks[j], lanes(2 * start + 256 * k + 128, 128)] = (
                        scaled_back * act
                    ).astype(BF16)
                gacc[j, 0:rows, :] = total

        def body(k, carry):
            tile(256 * k, 256)
            return carry

        lax.fori_loop(0, full_tiles, body, 0)
        if units % 256:
            tile(256 * full_tiles, 128)

    def scale(j):
        g = gcol[j][:, 0:1]
        scaled[blocks[j], :] = (g * c[blocks[j], :].astype(F32)).astype(BF16)

    def column(j, tile):
        gcol[j] = jnp.broadcast_to(tile.T[0:rows, 0:1], (rows, 128))

    base = 64

    def first(i, j):
        d = (z + 1 + i) % 4
        return pltpu.make_async_remote_copy(
            src_ref=part.at[blocks[j], lanes(chunk * d + size * (1 - core), size)],
            dst_ref=r1.at[4 * d + j],
            send_sem=send_sem.at[base + 4 * i + j],
            recv_sem=recv_sem.at[base + 4 * i + j],
            device_id=(me, other),
            device_id_type=MESH,
        )

    def grad_in(at, js):
        def body(i, carry):
            d = (z + 1 + i) % 4
            cols = lanes(chunk * d, chunk, 256)
            part[at, cols] = lax.dot_general(
                hcat[at, :], wcat[cols, :], NT, preferred_element_type=F32
            ).astype(BF16)
            for j in js:
                first(i, j).start()
            return carry

        lax.fori_loop(0, 4, body, 0)

    def second(i, j):
        d = (z + 1 + i) % 4
        return pltpu.make_async_remote_copy(
            src_ref=m.at[4 * d + j],
            dst_ref=r2.at[4 * d + j],
            send_sem=send_sem.at[base + 16 + 4 * i + j],
            recv_sem=recv_sem.at[base + 16 + 4 * i + j],
            device_id=(flip(me, j), t),
            device_id_type=MESH,
        )

    def merge(j):
        def body(i, carry):
            d = (z + 1 + i) % 4
            first(i, j).wait_recv()
            mine = part[blocks[j], lanes(chunk * d + size * core, size)].astype(F32)
            m[4 * d + j] = (mine + r1[4 * d + j].astype(F32)).astype(BF16)
            if j:
                second(i, j).start()
            return carry

        lax.fori_loop(0, 4, body, 0)

    def d_hidden(lo, hi):
        def body(i, carry):
            cols = lanes(256 * i, 256, 256)
            grads = lax.dot_general(
                x[:, cols], hcat[...], TN, preferred_element_type=F32
            ).astype(BF16)
            for k in range(units // 128):
                d_gate[cols, 128 * k : 128 * k + 128] = grads[:, 256 * k : 256 * k + 128]
                d_up[cols, 128 * k : 128 * k + 128] = grads[:, 256 * k + 128 : 256 * k + 256]
            return carry

        lax.fori_loop(lo, hi, body, 0)

    def d_out(lo, hi):
        def body(i, carry):
            cols = lanes(128 * i, 128)
            d_down[cols, :] = lax.dot_general(
                hid[:, cols], scaled[...], TN, preferred_element_type=F32
            ).astype(BF16)
            return carry

        lax.fori_loop(lo, hi, body, 0)

    column(0, gs[0])
    for copy in weights:
        copy.wait()
    gate_up(blocks[0], 1)
    pass_near(0, (0, 1))
    back_of(blocks[0], (0,))
    pass_near(0, (2, 3))
    scale(0)
    grad_in(blocks[0], (0,))
    pass_near(1, (0, 1))
    for copy in gate_in:
        copy.wait_recv()
    for j in (1, 2, 3):
        column(j, gin[j])
    merge(0)
    pass_near(1, (2, 3))
    pass_on(moved[0])
    pass_on(direct[0][0:2])
    for copy in landed[0][2:4] + landed[0][6:8]:
        copy.wait_recv()
    gate_up(blocks[3], 1)
    pass_on(direct[0][2:4])
    pass_on(moved[1][2:4])
    pass_on(direct[1][0:2])
    for copy in landed[0][0:2] + landed[0][4:6] + landed[0][8:12]:
        copy.wait_recv()
    pair = pl.ds(rows, 2 * rows)
    for copy in landed[1][2:4] + landed[1][4:6]:
        copy.wait_recv()
    back_of(blocks[3], (3,))
    scale(3)
    grad_in(blocks[3], (3,))
    pass_on(moved[1][0:2])
    pass_on(direct[1][2:4])
    gate_up(pair, 2)
    merge(3)
    for copy in landed[1][0:2] + landed[1][6:12]:
        copy.wait_recv()
    back_of(pair, (1, 2))
    scale(1)
    scale(2)
    for j in range(4):
        row = jnp.sum(gacc[j].T, axis=0, keepdims=True)
        gp[j] = jnp.broadcast_to(row, gp.shape[1:])
    stage = do.send(gp, rg.at[0], me, other)
    grad_in(pair, (1, 2))
    d_out(0, 2)
    merge(1)
    merge(2)
    stage.wait_recv()
    gt[0] = gp[...] + rg[0]
    stage = do.send(gt.at[0], rg.at[1], me, flip(t, 2))
    d_out(2, units // 128)
    stage.wait_recv()
    gt[1] = gt[0] + rg[1]
    stage = do.send(gt.at[1], rg.at[2], me, flip(t, 4))
    d_hidden(0, width // 1024)
    stage.wait_recv()
    gt[2] = gt[1] + rg[2]
    gate_back = [do.send(gt.at[2, j], go.at[j], flip(me, j), t) for j in (1, 2, 3)]
    d_hidden(width // 1024, width // 512)

    def gathered(i):
        d = (z + 1 + i) % 4
        total = m[4 * d].astype(F32)
        for j in (3, 1, 2):
            second(i, j).wait_recv()
            total = total + r2[4 * d + j].astype(F32)
        return total

    def third(i):
        d = (z + 1 + i) % 4
        return pltpu.make_async_remote_copy(
            src_ref=s.at[d],
            dst_ref=r3.at[i],
            send_sem=send_sem.at[base + 32 + i],
            recv_sem=recv_sem.at[base + 32 + i],
            device_id=(me, 2 * d + core),
            device_id_type=MESH,
        )

    for i in range(3):
        s[(z + 1 + i) % 4] = gathered(i).astype(BF16)
        third(i).start()
    total = gathered(3)
    d_hidden(width // 512, width // 256)
    for copy in gate_back:
        copy.wait_recv()
    sums = [gt[2, 0]] + [go[j] for j in (1, 2, 3)]
    picked = jnp.zeros(routing.shape, F32)
    for j in range(4):
        row = jnp.broadcast_to(sums[j][0:1, 0:rows], routing.shape)
        picked = jnp.where(routes == flip(me, j), row, picked)
    gates_out[...] = picked
    for i in range(3):
        third(i).wait_recv()
        total = total + r3[i].astype(F32)
    out[...] = total.astype(out.dtype)
    do.finish()
    for i in range(4):
        for j in range(4):
            first(i, j).wait_send()
            if j:
                second(i, j).wait_send()
        if i < 3:
            third(i).wait_send()


def dense(tokens, cotangent, routing, gate_weights, gate_proj, up_proj, down_proj):
    rows, width = tokens.shape
    units, parts = gate_proj.shape[2], lax.axis_size("tp")
    size = width // parts
    top_k = routing.shape[1]
    vmem, anywhere = pl.BlockSpec(memory_space=pltpu.VMEM), pl.BlockSpec(memory_space=pl.ANY)
    shape = jax.ShapeDtypeStruct
    tile = pltpu.VMEM((16, rows, size), BF16)
    flat = (4, 8, 256)
    grad_tokens, grad_gates, d_gate, d_up, d_down = pl.pallas_call(
        layer_kernel,
        out_shape=[
            shape((rows, size), BF16),
            shape((top_k, rows), F32),
            shape((width, units), BF16),
            shape((width, units), BF16),
            shape((units, width), BF16),
        ],
        in_specs=[anywhere, anywhere, vmem, vmem, anywhere, anywhere, anywhere],
        out_specs=[vmem] * 5,
        scratch_shapes=[
            pltpu.VMEM((4 * rows, width), BF16),
            pltpu.VMEM((4 * rows, width), BF16),
            pltpu.VMEM((4 * rows, width), BF16),
            pltpu.VMEM((width, 2 * units), BF16),
            pltpu.VMEM((units, width), BF16),
            pltpu.VMEM((4 * rows, 2 * units), F32),
            pltpu.VMEM((4 * rows, 2 * units), BF16),
            pltpu.VMEM((4 * rows, units), BF16),
            pltpu.VMEM((4 * rows, width), BF16),
            pltpu.VMEM(flat, F32),
            pltpu.VMEM(flat, F32),
            pltpu.VMEM((4, rows, 128), F32),
            pltpu.VMEM((4, 256, 128), F32),
            tile,
            tile,
            tile,
            pltpu.VMEM((4, rows, size), BF16),
            pltpu.VMEM((3, rows, size), BF16),
            pltpu.VMEM(flat, F32),
            pltpu.VMEM((3,) + flat, F32),
            pltpu.VMEM((3,) + flat, F32),
            pltpu.VMEM(flat, F32),
            pltpu.SemaphoreType.DMA((104,)),
            pltpu.SemaphoreType.DMA((104,)),
            pltpu.SemaphoreType.DMA((3 + 2 * (units // 128),)),
        ],
        compiler_params=pltpu.CompilerParams(
            collective_id=0, has_side_effects=True, vmem_limit_bytes=62 << 20
        ),
    )(tokens, cotangent, routing.T, gate_weights.T, gate_proj[0], up_proj[0], down_proj[0])
    return grad_tokens, grad_gates.T, d_gate[None], d_up[None], d_down[None]


def local(tokens, cotangent, routing, gate_weights, gate_proj, up_proj, down_proj):
    experts, parts = lax.axis_size("ep"), lax.axis_size("tp")
    capacity = 2 * tokens.shape[0] * routing.shape[1] // experts
    fits = experts == 4 and parts == 8 and tokens.shape[1] % 1024 == 0
    fits = fits and tokens.shape[0] % 16 == 0 and tokens.shape[0] <= 256
    fits = fits and gate_proj.shape[2] % 128 == 0
    plan = dense if capacity >= tokens.shape[0] and fits else slotted
    return plan(tokens, cotangent, routing, gate_weights, gate_proj, up_proj, down_proj)


def solution(mesh):
    return jax.shard_map(
        local,
        mesh=mesh,
        in_specs=(
            P("ep", None),
            P("ep", None),
            P("ep", None),
            P("ep", None),
            P("ep", None, "tp"),
            P("ep", None, "tp"),
            P("ep", "tp", None),
        ),
        out_specs=(
            P("ep", "tp"),
            P("ep", None),
            P("ep", None, "tp"),
            P("ep", None, "tp"),
            P("ep", "tp", None),
        ),
        check_vma=False,
    )
```

time: 114 us -> 84.9 us (0.74)
  matrix products: 45.9 us -> 0 us
  Pallas kernels: 62.1 us -> 71.7 us
  local copies, waits for them, and re-layouts: 3.16 us -> 12.3 us
  other arithmetic: 1.33 us -> 0 us
    dot_general x8 -> x0, matrix products: 45.9 us -> none  [the longest x1 9.28 us: expert_backward(): up_value = jnp.dot(in_rows, w_up, preferred_element_type=jnp.float32)]
    pallas_call x2 -> x1, Pallas kernels: 62.1 us -> 71.7 us  [dense(): pl.pallas_call(layer_kernel, out_shape=[shape((rows, size), BF16), shape(...]
    unnamed x29 -> x9, local copies, waits for them, and re-layouts: 2.96 us -> 12.3 us
where the time goes in v1:
time: 84.9 us; the launch traced here: 84.6 us
  Pallas kernels  71.7 us (84%)
  local copies, waits for them, and re-layouts  12.3 us (14%)
    pallas_call x1, Pallas kernels, dense(): pl.pallas_call(layer_kernel, out_shape=[shape((rows, size), BF16), shape(...  71.7 us
    unnamed x9, local copies, waits for them, and re-layouts  12.3 us

profile of v1, /device:TPU:0, one launch (start us, length us, event | category | flops | bytes accessed | tf_op | source)
XLA Modules:
  0.0 84.6 jit_solution(1371417499383850337)
XLA Ops:
  0.6 71.7 %shard_map.110 = (bf16[192,256]{1,0:T(8,128)(2,1)}, f32[2,192]{1,0:T(2,128)}, bf16[2048,896]{1,0:T(8,128)(2,1)}, bf16[2048,896]{1,0:T(8,128)(2,1)}, bf16[896,2048]{1,0:T(8,128)(2,1)}) custom-call(bf16[192,2048]{1,0:T(8,128)(2,1)} %tok.1, bf16[192,2048]{1,0:T(8,128)(2,1)} %cot.1, s32[2,192]{1,0:T(2,128)} %bitcast.16, bf16[2,192]{1,0:T(2,128)(2,1)} %bitcast.17, ...), custom_call_target="tpu_custom_call" | custom-call | tf_op jit(solution)/shard_map/pallas_call | solution.py:498
  72.3 1.5 %copy.17 = bf16[192,256]{1,0:T(8,128)(2,1)} copy(bf16[192,256]{1,0:T(8,128)(2,1)} %get-tuple-element.20) | data formatting | bytes 196608
  73.8 1.3 %copy.18 = f32[192,2]{0,1:T(2,128)} copy(f32[192,2]{0,1:T(2,128)} %bitcast.15) | data formatting | bytes 3072
  75.1 0.0 copy-start.1
  75.1 4.3 %copy.19 = bf16[1,2048,896]{2,1,0:T(8,128)(2,1)} copy(bf16[1,2048,896]{2,1,0:T(8,128)(2,1)} %bitcast.11) | data formatting | bytes 7340032
  79.4 0.0 copy-done.1
  79.4 0.0 copy-start
  79.4 1.9 %copy.20 = bf16[1,2048,896]{2,1,0:T(8,128)(2,1)} copy(bf16[1,2048,896]{2,1,0:T(8,128)(2,1)S(1)} %bitcast.10) | data formatting | bytes 7340032
  81.3 1.5 %copy-done = bf16[896,2048]{1,0:T(8,128)(2,1)S(1)} copy-done((bf16[896,2048]{1,0:T(8,128)(2,1)S(1)}, bf16[896,2048]{1,0:T(8,128)(2,1)}, u32[]{:S(2)}) %copy-start) | copy-done | bytes 3670040
  82.8 1.8 %copy.21 = bf16[1,896,2048]{2,1,0:T(8,128)(2,1)} copy(bf16[1,896,2048]{2,1,0:T(8,128)(2,1)S(1)} %bitcast.9) | data formatting | bytes 7340032
Async XLA Ops:
  75.1 4.3 %copy-start.1 = (bf16[2048,896]{1,0:T(8,128)(2,1)S(1)}, bf16[2048,896]{1,0:T(8,128)(2,1)}, u32[]{:S(2)}) copy-start(bf16[2048,896]{1,0:T(8,128)(2,1)} %get-tuple-element.13) | copy-start | bytes 11010052
  79.4 3.4 %copy-start = (bf16[896,2048]{1,0:T(8,128)(2,1)S(1)}, bf16[896,2048]{1,0:T(8,128)(2,1)}, u32[]{:S(2)}) copy-start(bf16[896,2048]{1,0:T(8,128)(2,1)} %get-tuple-element.14) | copy-start | bytes 11010052

commit v2 on v1

--- a/solution.py
+++ b/solution.py
@@ -164,8 +164,8 @@
 def layer_kernel(
     tok, cot, routing, gates, w_gate, w_up, w_down,
     out, gates_out, d_gate, d_up, d_down,
-    x, c, scaled, wcat, wd, pu, hcat, hid, part,
-    gs, gin, gcol, gacc, r1, m, r2, s, r3, gp, rg, gt, go,
+    routes_in, weight_in, x, c, scaled, wcat, wd, pu, hcat, hid, part,
+    gs, gin, gcol, gacc, r1, m, r2, r4, s, r3, gp, rg, gt, go,
     send_sem, recv_sem, own_sem,
 ):
     me, t = lax.axis_index("ep"), lax.axis_index("tp")
@@ -183,8 +183,13 @@
 
     n = 0
     loads = []
-    for src, dst in ((tok, x), (cot, c)):
-        loads.append(pltpu.make_async_copy(src, dst.at[blocks[0]], own_sem.at[n]))
+    for src, dst in (
+        (tok, x.at[blocks[0]]),
+        (cot, c.at[blocks[0]]),
+        (routing, routes_in),
+        (gates, weight_in),
+    ):
+        loads.append(pltpu.make_async_copy(src, dst, own_sem.at[n]))
         n += 1
     weights = []
     for k in range(units // 128):
@@ -208,15 +213,15 @@
 
     gs[...] = jnp.zeros_like(gs)
     gacc[...] = jnp.zeros_like(gacc)
-    routes, weight = routing[...], gates[...].astype(F32)
+    for copy in loads:
+        copy.wait()
+    routes, weight = routes_in[...], weight_in[...].astype(F32)
     for j in range(4):
         row = jnp.sum(jnp.where(routes == flip(me, j), weight, 0.0), axis=0, keepdims=True)
         gs[j, :, 0:rows] = jnp.broadcast_to(row, (8, rows))
     pl.semaphore_wait(barrier, len(partners))
 
     do = Copies(send_sem, recv_sem)
-    for copy in loads:
-        copy.wait()
     gate_in = [do.send(gs.at[j], gin.at[j], flip(me, j), t) for j in (1, 2, 3)]
 
     def ep_send(a, j, cols):
@@ -231,27 +236,31 @@
     low, high = lanes(quarter * q, eighth), lanes(quarter * q + eighth, eighth)
     far_low, far_high = lanes(quarter * far, eighth), lanes(quarter * far + eighth, eighth)
     both = (x, c)
-    near, direct = {}, {}
-    for ref in (0, 1):
-        near[ref] = [ep_send(ref, 1, high), ep_send(ref, 2, high)]
-        near[ref] += [ep_send(ref, 3, low), ep_send(ref, 3, high)]
-    for ref in (0, 1):
-        direct[ref] = [ep_send(ref, j, w) for w in (low, far_low) for j in (1, 2)]
-    mirror = [far_high, far_high, far_low, far_high]
-    moved = ([], [])
-    landed = ([], [])
-
-    def pass_near(ref, part_of):
-        for n in part_of:
-            item = near[ref][n]
-            item[0].wait_recv()
-            moved[ref].append((relay(item, 2), ref, item[2], mirror[n]))
-            landed[ref].append(relay(item, 1))
+    lead, rest, wide = {}, {}, {}
+    landed = {0: [], 1: [], 2: [], 3: []}
+
+    def over_ep(item, j):
+        _, a, _, cols = item
+        src = both[a].at[blocks[item[2]], cols]
+        copy = do.send(src, both[a].at[blocks[3], cols], flip(me, j), t)
+        return (copy, a, 3, cols)
+
+    def over_z(item, mirror):
+        return (relay(item, 2), item[1], item[2], mirror)
 
     def pass_on(items):
         for item in items:
             item[0].wait_recv()
-            landed[item[1]].append(relay(item, 1))
+            landed[item[2]].append((item[1], relay(item, 1)))
+
+    def complete(j, a):
+        for kind, copy in landed[j]:
+            if kind == a:
+                copy.wait_recv()
+
+    for a in (0, 1):
+        lead[a] = [ep_send(a, 1, low), ep_send(a, 2, high)]
+    rest[0] = [ep_send(0, 1, high), ep_send(0, 2, low)]
 
     def gate_up(at, count):
         def tile(start, size_of):
@@ -343,6 +352,32 @@
             device_id_type=MESH,
         )
 
+    def fourth(d):
+        return pltpu.make_async_remote_copy(
+            src_ref=m.at[4 * d + 3],
+            dst_ref=r4.at[d // 2],
+            send_sem=send_sem.at[base + 36 + d],
+            recv_sem=recv_sem.at[base + 36 + d],
+            device_id=(me, flip(t, 2)),
+            device_id_type=MESH,
+        )
+
+    def merge_diagonal():
+        for i in (0, 2, 1, 3):
+            d = (z + 1 + i) % 4
+            first(i, 3).wait_recv()
+            mine = part[blocks[3], lanes(chunk * d + size * core, size)].astype(F32)
+            m[4 * d + 3] = (mine + r1[4 * d + 3].astype(F32)).astype(BF16)
+            if i % 2 == 0:
+                fourth(d).start()
+
+    def send_diagonal():
+        for i in (1, 3):
+            d = (z + 1 + i) % 4
+            fourth(d).wait_recv()
+            m[4 * d + 3] = (m[4 * d + 3].astype(F32) + r4[d // 2].astype(F32)).astype(BF16)
+            second(i, 3).start()
+
     def merge(j):
         def body(i, carry):
             d = (z + 1 + i) % 4
@@ -382,55 +417,67 @@
     for copy in weights:
         copy.wait()
     gate_up(blocks[0], 1)
-    pass_near(0, (0, 1))
+    pass_on(lead[0])
+    diag = {0: [over_ep(lead[0][0], 2), over_ep(lead[0][1], 1)]}
+    crossed = {0: [over_z(lead[0][0], far_low), over_z(lead[0][1], far_high)]}
     back_of(blocks[0], (0,))
-    pass_near(0, (2, 3))
+    pass_on(lead[1])
+    diag[1] = [over_ep(lead[1][0], 2), over_ep(lead[1][1], 1)]
+    crossed[1] = [over_z(lead[1][0], far_low)]
+    wide[0] = [ep_send(0, 1, far_high), ep_send(0, 2, far_low)]
+    rest[1] = [ep_send(1, 1, high), ep_send(1, 2, low)]
+    wide[1] = [ep_send(1, 1, far_high), ep_send(1, 2, far_low)]
     scale(0)
     grad_in(blocks[0], (0,))
-    pass_near(1, (0, 1))
+    pass_on(rest[0])
+    pass_on(crossed[0])
+    pass_on(diag[0])
+    across = {0: [over_z(diag[0][0], far_low), over_z(diag[0][1], far_high)]}
+    merge(0)
     for copy in gate_in:
         copy.wait_recv()
     for j in (1, 2, 3):
         column(j, gin[j])
-    merge(0)
-    pass_near(1, (2, 3))
-    pass_on(moved[0])
-    pass_on(direct[0][0:2])
-    for copy in landed[0][2:4] + landed[0][6:8]:
-        copy.wait_recv()
+    pass_on(diag[1])
+    across[1] = [over_z(diag[1][0], far_low), over_z(diag[1][1], far_high)]
+    crossed[1].append(over_z(lead[1][1], far_high))
+    pass_on(wide[0])
+    pass_on(crossed[1][0:1])
+    complete(1, 0)
+    complete(2, 0)
+    pair = pl.ds(rows, 2 * rows)
+    gate_up(pair, 2)
+    pass_on(rest[1])
+    pass_on(across[0])
+    complete(3, 0)
     gate_up(blocks[3], 1)
-    pass_on(direct[0][2:4])
-    pass_on(moved[1][2:4])
-    pass_on(direct[1][0:2])
-    for copy in landed[0][0:2] + landed[0][4:6] + landed[0][8:12]:
-        copy.wait_recv()
-    pair = pl.ds(rows, 2 * rows)
-    for copy in landed[1][2:4] + landed[1][4:6]:
-        copy.wait_recv()
+    pass_on(wide[1])
+    complete(1, 1)
+    back_of(blocks[1], (1,))
+    scale(1)
+    pass_on(across[1])
+    complete(3, 1)
     back_of(blocks[3], (3,))
     scale(3)
+    pass_on(crossed[1][1:2])
     grad_in(blocks[3], (3,))
-    pass_on(moved[1][0:2])
-    pass_on(direct[1][2:4])
-    gate_up(pair, 2)
-    merge(3)
-    for copy in landed[1][0:2] + landed[1][6:12]:
-        copy.wait_recv()
-    back_of(pair, (1, 2))
-    scale(1)
+    complete(2, 1)
+    back_of(blocks[2], (2,))
+    merge_diagonal()
+    grad_in(pair, (1, 2))
+    send_diagonal()
     scale(2)
+    merge(1)
+    merge(2)
     for j in range(4):
         row = jnp.sum(gacc[j].T, axis=0, keepdims=True)
         gp[j] = jnp.broadcast_to(row, gp.shape[1:])
     stage = do.send(gp, rg.at[0], me, other)
-    grad_in(pair, (1, 2))
-    d_out(0, 2)
-    merge(1)
-    merge(2)
+    d_out(0, 3)
     stage.wait_recv()
     gt[0] = gp[...] + rg[0]
     stage = do.send(gt.at[0], rg.at[1], me, flip(t, 2))
-    d_out(2, units // 128)
+    d_out(3, units // 128)
     stage.wait_recv()
     gt[1] = gt[0] + rg[1]
     stage = do.send(gt.at[1], rg.at[2], me, flip(t, 4))
@@ -438,12 +485,11 @@
     stage.wait_recv()
     gt[2] = gt[1] + rg[2]
     gate_back = [do.send(gt.at[2, j], go.at[j], flip(me, j), t) for j in (1, 2, 3)]
-    d_hidden(width // 1024, width // 512)
 
     def gathered(i):
         d = (z + 1 + i) % 4
         total = m[4 * d].astype(F32)
-        for j in (3, 1, 2):
+        for j in (3, 1, 2) if i % 2 else (1, 2):
             second(i, j).wait_recv()
             total = total + r2[4 * d + j].astype(F32)
         return total
@@ -462,8 +508,8 @@
     for i in range(3):
         s[(z + 1 + i) % 4] = gathered(i).astype(BF16)
         third(i).start()
+    d_hidden(width // 1024, width // 256)
     total = gathered(3)
-    d_hidden(width // 512, width // 256)
     for copy in gate_back:
         copy.wait_recv()
     sums = [gt[2, 0]] + [go[j] for j in (1, 2, 3)]
@@ -480,10 +526,27 @@
     for i in range(4):
         for j in range(4):
             first(i, j).wait_send()
-            if j:
+            if j in (1, 2) or (j and i % 2):
                 second(i, j).wait_send()
+        if i % 2 == 0:
+            fourth((z + 1 + i) % 4).wait_send()
         if i < 3:
             third(i).wait_send()
+
+
+def store_kernel(*refs):
+    sources, targets, sem = refs[0:5], refs[5:10], refs[10]
+    copies = []
+    for a, (src, dst) in enumerate(zip(sources, targets)):
+        parts = 4 if src.shape[0] % 512 == 0 or src.shape[0] > 512 else 1
+        step = src.shape[0] // parts
+        for k in range(parts):
+            piece = pl.ds(k * step, step)
+            copies.append(pltpu.make_async_copy(src.at[piece], dst.at[piece], sem.at[a, k]))
+    for copy in copies:
+        copy.start()
+    for copy in copies:
+        copy.wait()
 
 
 def dense(tokens, cotangent, routing, gate_weights, gate_proj, up_proj, down_proj):
@@ -491,22 +554,24 @@
     units, parts = gate_proj.shape[2], lax.axis_size("tp")
     size = width // parts
     top_k = routing.shape[1]
-    vmem, anywhere = pl.BlockSpec(memory_space=pltpu.VMEM), pl.BlockSpec(memory_space=pl.ANY)
+    vmem, hbm = pl.BlockSpec(memory_space=pltpu.VMEM), pl.BlockSpec(memory_space=pltpu.HBM)
     shape = jax.ShapeDtypeStruct
     tile = pltpu.VMEM((16, rows, size), BF16)
     flat = (4, 8, 256)
-    grad_tokens, grad_gates, d_gate, d_up, d_down = pl.pallas_call(
+    results = pl.pallas_call(
         layer_kernel,
         out_shape=[
-            shape((rows, size), BF16),
-            shape((top_k, rows), F32),
-            shape((width, units), BF16),
-            shape((width, units), BF16),
-            shape((units, width), BF16),
+            pltpu.VMEM((rows, size), BF16),
+            pltpu.VMEM((top_k, rows), F32),
+            pltpu.VMEM((width, units), BF16),
+            pltpu.VMEM((width, units), BF16),
+            pltpu.VMEM((units, width), BF16),
         ],
-        in_specs=[anywhere, anywhere, vmem, vmem, anywhere, anywhere, anywhere],
+        in_specs=[hbm] * 7,
         out_specs=[vmem] * 5,
         scratch_shapes=[
+            pltpu.VMEM((top_k, rows), routing.dtype),
+            pltpu.VMEM((top_k, rows), gate_weights.dtype),
             pltpu.VMEM((4 * rows, width), BF16),
             pltpu.VMEM((4 * rows, width), BF16),
             pltpu.VMEM((4 * rows, width), BF16),
@@ -523,6 +588,7 @@
             tile,
             tile,
             tile,
+            pltpu.VMEM((2, rows, size), BF16),
             pltpu.VMEM((4, rows, size), BF16),
             pltpu.VMEM((3, rows, size), BF16),
             pltpu.VMEM(flat, F32),
@@ -531,12 +597,33 @@
             pltpu.VMEM(flat, F32),
             pltpu.SemaphoreType.DMA((104,)),
             pltpu.SemaphoreType.DMA((104,)),
-            pltpu.SemaphoreType.DMA((3 + 2 * (units // 128),)),
+            pltpu.SemaphoreType.DMA((5 + 2 * (units // 128),)),
         ],
         compiler_params=pltpu.CompilerParams(
-            collective_id=0, has_side_effects=True, vmem_limit_bytes=62 << 20
+            collective_id=0, has_side_effects=True, vmem_limit_bytes=42 << 20
         ),
-    )(tokens, cotangent, routing.T, gate_weights.T, gate_proj[0], up_proj[0], down_proj[0])
+    )(
+        *(
+            pltpu.with_memory_space_constraint(a, pltpu.HBM)
+            for a in (
+                tokens,
+                cotangent,
+                routing.T,
+                gate_weights.T,
+                gate_proj[0],
+                up_proj[0],
+                down_proj[0],
+            )
+        )
+    )
+    grad_tokens, grad_gates, d_gate, d_up, d_down = pl.pallas_call(
+        store_kernel,
+        out_shape=[shape(r.shape, r.dtype) for r in results],
+        in_specs=[vmem] * 5,
+        out_specs=[hbm] * 5,
+        scratch_shapes=[pltpu.SemaphoreType.DMA((5, 4))],
+        compiler_params=pltpu.CompilerParams(vmem_limit_bytes=1 << 20),
+    )(*results)
     return grad_tokens, grad_gates.T, d_gate[None], d_up[None], d_down[None]
 
 

time: 84.9 us -> 71.3 us (0.84)
  local copies, waits for them, and re-layouts: 12.3 us -> 0 us
  Pallas kernels: 71.7 us -> 70.5 us
    unnamed x9 -> x0, local copies, waits for them, and re-layouts: 12.3 us -> none
    pallas_call x1 -> x2, Pallas kernels: 71.7 us -> 70.5 us  [the longest x1 66.2 us: dense(): pl.pallas_call(layer_kernel, out_shape=[pltpu.VMEM((rows, size), BF16), p...]
where the time goes in v2:
time: 71.3 us; the launch traced here: 71.1 us
  Pallas kernels  70.5 us (99%)
    pallas_call x1, Pallas kernels, dense(): pl.pallas_call(layer_kernel, out_shape=[pltpu.VMEM((rows, size), BF16), p...  66.2 us
    pallas_call x1, Pallas kernels, dense(): pl.pallas_call(store_kernel, out_shape=[shape(r.shape, r.dtype) for r in...  4.3 us

profile of v2, /device:TPU:0, one launch (start us, length us, event | category | flops | bytes accessed | tf_op | source)
XLA Modules:
  0.0 71.1 jit_solution(10634302031129884024)
XLA Ops:
  0.6 66.2 %shard_map.110 = (bf16[192,256]{1,0:T(8,128)(2,1)S(1)}, f32[2,192]{1,0:T(2,128)S(1)}, bf16[2048,896]{1,0:T(8,128)(2,1)S(1)}, bf16[2048,896]{1,0:T(8,128)(2,1)S(1)}, bf16[896,2048]{1,0:T(8,128)(2,1)S(1)}) custom-call(bf16[192,2048]{1,0:T(8,128)(2,1)} %tok.1, bf16[192,2048]{1,0:T(8,128)(2,1)} %cot.1, s32[2,192]{1,0:T(2,128)} %bitcast.12, ...), custom_call_target="tpu_custom_call" | custom-call | tf_op jit(solution)/shard_map/pallas_call | solution.py:561
  66.8 4.3 %shard_map.111 = (bf16[192,256]{1,0:T(8,128)(2,1)}, f32[2,192]{1,0:T(2,128)}, bf16[2048,896]{1,0:T(8,128)(2,1)}, bf16[2048,896]{1,0:T(8,128)(2,1)}, bf16[896,2048]{1,0:T(8,128)(2,1)}) custom-call(bf16[192,256]{1,0:T(8,128)(2,1)S(1)} %get-tuple-element.15.refs_0_, f32[2,192]{1,0:T(2,128)S(1)} %get-tuple-element.16.refs_1_, ...), custom_call_target="tpu_custom_call" | custom-call | tf_op jit(solution)/shard_map/pallas_call | solution.py:619

commit v3 on v2

--- a/solution.py
+++ b/solution.py
@@ -203,7 +203,7 @@
             )
             n += 1
     weights.append(pltpu.make_async_copy(w_down, wd, own_sem.at[n]))
-    for copy in loads + weights:
+    for copy in loads:
         copy.start()
 
     barrier = pltpu.get_barrier_semaphore()
@@ -215,6 +215,8 @@
     gacc[...] = jnp.zeros_like(gacc)
     for copy in loads:
         copy.wait()
+    for copy in weights:
+        copy.start()
     routes, weight = routes_in[...], weight_in[...].astype(F32)
     for j in range(4):
         row = jnp.sum(jnp.where(routes == flip(me, j), weight, 0.0), axis=0, keepdims=True)
@@ -258,9 +260,9 @@
             if kind == a:
                 copy.wait_recv()
 
-    for a in (0, 1):
-        lead[a] = [ep_send(a, 1, low), ep_send(a, 2, high)]
+    lead[0] = [ep_send(0, 1, low), ep_send(0, 2, high)]
     rest[0] = [ep_send(0, 1, high), ep_send(0, 2, low)]
+    wide[0] = [ep_send(0, 1, far_high), ep_send(0, 2, far_low)]
 
     def gate_up(at, count):
         def tile(start, size_of):
@@ -271,7 +273,7 @@
             tile(512 * k, 512)
             return carry
 
-        lax.fori_loop(0, full_tiles, body, 0)
+        lax.fori_loop(0, full_tiles, body, 0, unroll=True)
         if units % 256:
             tile(512 * full_tiles, 256)
 
@@ -304,7 +306,7 @@
             tile(256 * k, 256)
             return carry
 
-        lax.fori_loop(0, full_tiles, body, 0)
+        lax.fori_loop(0, full_tiles, body, 0, unroll=True)
         if units % 256:
             tile(256 * full_tiles, 128)
 
@@ -328,19 +330,6 @@
             device_id_type=MESH,
         )
 
-    def grad_in(at, js):
-        def body(i, carry):
-            d = (z + 1 + i) % 4
-            cols = lanes(chunk * d, chunk, 256)
-            part[at, cols] = lax.dot_general(
-                hcat[at, :], wcat[cols, :], NT, preferred_element_type=F32
-            ).astype(BF16)
-            for j in js:
-                first(i, j).start()
-            return carry
-
-        lax.fori_loop(0, 4, body, 0)
-
     def second(i, j):
         d = (z + 1 + i) % 4
         return pltpu.make_async_remote_copy(
@@ -362,15 +351,6 @@
             device_id_type=MESH,
         )
 
-    def merge_diagonal():
-        for i in (0, 2, 1, 3):
-            d = (z + 1 + i) % 4
-            first(i, 3).wait_recv()
-            mine = part[blocks[3], lanes(chunk * d + size * core, size)].astype(F32)
-            m[4 * d + 3] = (mine + r1[4 * d + 3].astype(F32)).astype(BF16)
-            if i % 2 == 0:
-                fourth(d).start()
-
     def send_diagonal():
         for i in (1, 3):
             d = (z + 1 + i) % 4
@@ -378,17 +358,32 @@
             m[4 * d + 3] = (m[4 * d + 3].astype(F32) + r4[d // 2].astype(F32)).astype(BF16)
             second(i, 3).start()
 
-    def merge(j):
-        def body(i, carry):
+    def merge(i, j):
+        d = (z + 1 + i) % 4
+        first(i, j).wait_recv()
+        mine = part[blocks[j], lanes(chunk * d + size * core, size)].astype(F32)
+        m[4 * d + j] = (mine + r1[4 * d + j].astype(F32)).astype(BF16)
+        if j == 3 and i % 2 == 0:
+            fourth(d).start()
+        elif j in (1, 2):
+            second(i, j).start()
+
+    def grad_in(at, js, merged=(), step=None, hook=None):
+        for i in range(4):
             d = (z + 1 + i) % 4
-            first(i, j).wait_recv()
-            mine = part[blocks[j], lanes(chunk * d + size * core, size)].astype(F32)
-            m[4 * d + j] = (mine + r1[4 * d + j].astype(F32)).astype(BF16)
-            if j:
-                second(i, j).start()
-            return carry
-
-        lax.fori_loop(0, 4, body, 0)
+            cols = lanes(chunk * d, chunk, 256)
+            part[at, cols] = lax.dot_general(
+                hcat[at, :], wcat[cols, :], NT, preferred_element_type=F32
+            ).astype(BF16)
+            for j in js:
+                first(i, j).start()
+            if i:
+                for j in merged:
+                    merge(i - 1, j)
+            if i == step:
+                hook()
+        for j in merged:
+            merge(3, j)
 
     def d_hidden(lo, hi):
         def body(i, carry):
@@ -401,7 +396,7 @@
                 d_up[cols, 128 * k : 128 * k + 128] = grads[:, 256 * k + 128 : 256 * k + 256]
             return carry
 
-        lax.fori_loop(lo, hi, body, 0)
+        lax.fori_loop(lo, hi, body, 0, unroll=2)
 
     def d_out(lo, hi):
         def body(i, carry):
@@ -411,7 +406,7 @@
             ).astype(BF16)
             return carry
 
-        lax.fori_loop(lo, hi, body, 0)
+        lax.fori_loop(lo, hi, body, 0, unroll=2)
 
     column(0, gs[0])
     for copy in weights:
@@ -420,71 +415,52 @@
     pass_on(lead[0])
     diag = {0: [over_ep(lead[0][0], 2), over_ep(lead[0][1], 1)]}
     crossed = {0: [over_z(lead[0][0], far_low), over_z(lead[0][1], far_high)]}
+    lead[1] = [ep_send(1, 1, low), ep_send(1, 2, high)]
+    wide[1] = [ep_send(1, 1, far_high), ep_send(1, 2, far_low)]
+    rest[1] = [ep_send(1, 1, high), ep_send(1, 2, low)]
     back_of(blocks[0], (0,))
-    pass_on(lead[1])
-    diag[1] = [over_ep(lead[1][0], 2), over_ep(lead[1][1], 1)]
-    crossed[1] = [over_z(lead[1][0], far_low)]
-    wide[0] = [ep_send(0, 1, far_high), ep_send(0, 2, far_low)]
-    rest[1] = [ep_send(1, 1, high), ep_send(1, 2, low)]
-    wide[1] = [ep_send(1, 1, far_high), ep_send(1, 2, far_low)]
-    scale(0)
-    grad_in(blocks[0], (0,))
     pass_on(rest[0])
+    pass_on(wide[0])
+    grad_in(blocks[0], (0,), (0,))
     pass_on(crossed[0])
     pass_on(diag[0])
     across = {0: [over_z(diag[0][0], far_low), over_z(diag[0][1], far_high)]}
-    merge(0)
     for copy in gate_in:
         copy.wait_recv()
     for j in (1, 2, 3):
         column(j, gin[j])
-    pass_on(diag[1])
-    across[1] = [over_z(diag[1][0], far_low), over_z(diag[1][1], far_high)]
-    crossed[1].append(over_z(lead[1][1], far_high))
-    pass_on(wide[0])
-    pass_on(crossed[1][0:1])
+    scale(0)
+    pass_on(lead[1])
+    diag[1] = [over_ep(lead[1][0], 2), over_ep(lead[1][1], 1)]
+    crossed[1] = [over_z(lead[1][0], far_low), over_z(lead[1][1], far_high)]
     complete(1, 0)
     complete(2, 0)
     pair = pl.ds(rows, 2 * rows)
     gate_up(pair, 2)
+    pass_on(wide[1])
+    diag[1] += [over_ep(wide[1][0], 2), over_ep(wide[1][1], 1)]
     pass_on(rest[1])
     pass_on(across[0])
     complete(3, 0)
     gate_up(blocks[3], 1)
-    pass_on(wide[1])
+    pass_on(crossed[1][0:1])
     complete(1, 1)
     back_of(blocks[1], (1,))
-    scale(1)
-    pass_on(across[1])
+    pass_on(diag[1])
+    pass_on(crossed[1][1:2])
     complete(3, 1)
     back_of(blocks[3], (3,))
-    scale(3)
-    pass_on(crossed[1][1:2])
-    grad_in(blocks[3], (3,))
+    grad_in(blocks[3], (3,), (3,))
     complete(2, 1)
     back_of(blocks[2], (2,))
-    merge_diagonal()
-    grad_in(pair, (1, 2))
-    send_diagonal()
-    scale(2)
-    merge(1)
-    merge(2)
+    grad_in(pair, (1, 2), (1, 2), 2, send_diagonal)
+    for j in (1, 2, 3):
+        scale(j)
     for j in range(4):
         row = jnp.sum(gacc[j].T, axis=0, keepdims=True)
         gp[j] = jnp.broadcast_to(row, gp.shape[1:])
     stage = do.send(gp, rg.at[0], me, other)
-    d_out(0, 3)
-    stage.wait_recv()
-    gt[0] = gp[...] + rg[0]
-    stage = do.send(gt.at[0], rg.at[1], me, flip(t, 2))
-    d_out(3, units // 128)
-    stage.wait_recv()
-    gt[1] = gt[0] + rg[1]
-    stage = do.send(gt.at[1], rg.at[2], me, flip(t, 4))
-    d_hidden(0, width // 1024)
-    stage.wait_recv()
-    gt[2] = gt[1] + rg[2]
-    gate_back = [do.send(gt.at[2, j], go.at[j], flip(me, j), t) for j in (1, 2, 3)]
+    d_out(0, 4)
 
     def gathered(i):
         d = (z + 1 + i) % 4
@@ -505,11 +481,27 @@
             device_id_type=MESH,
         )
 
-    for i in range(3):
+    def pass_third(i):
         s[(z + 1 + i) % 4] = gathered(i).astype(BF16)
         third(i).start()
-    d_hidden(width // 1024, width // 256)
+
+    stage.wait_recv()
+    gt[0] = gp[...] + rg[0]
+    stage = do.send(gt.at[0], rg.at[1], me, flip(t, 2))
+    pass_third(0)
+    d_out(4, units // 128)
+    stage.wait_recv()
+    gt[1] = gt[0] + rg[1]
+    stage = do.send(gt.at[1], rg.at[2], me, flip(t, 4))
+    pass_third(1)
+    d_hidden(0, width // 1024)
+    stage.wait_recv()
+    gt[2] = gt[1] + rg[2]
+    gate_back = [do.send(gt.at[2, j], go.at[j], flip(me, j), t) for j in (1, 2, 3)]
+    pass_third(2)
+    d_hidden(width // 1024, width // 512)
     total = gathered(3)
+    d_hidden(width // 512, width // 256)
     for copy in gate_back:
         copy.wait_recv()
     sums = [gt[2, 0]] + [go[j] for j in (1, 2, 3)]

time: 71.3 us -> 68.2 us (0.957)
  Pallas kernels: 70.5 us -> 67.3 us
    pallas_call x1, Pallas kernels: 66.2 us -> 63 us  [dense(): pl.pallas_call(layer_kernel, out_shape=[pltpu.VMEM((rows, size), BF16), p...]
where the time goes in v3:
time: 68.2 us; the launch traced here: 68.1 us
  Pallas kernels  67.3 us (99%)
  between operations  0.8 us (1%)
    pallas_call x1, Pallas kernels, dense(): pl.pallas_call(layer_kernel, out_shape=[pltpu.VMEM((rows, size), BF16), p...  63 us
    pallas_call x1, Pallas kernels, dense(): pl.pallas_call(store_kernel, out_shape=[shape(r.shape, r.dtype) for r in...  4.3 us

profile of v3, /device:TPU:0, one launch (start us, length us, event | category | flops | bytes accessed | tf_op | source)
XLA Modules:
  0.0 68.1 jit_solution(7347992001056300677)
XLA Ops:
  0.6 63.0 %shard_map.110 = (bf16[192,256]{1,0:T(8,128)(2,1)S(1)}, f32[2,192]{1,0:T(2,128)S(1)}, bf16[2048,896]{1,0:T(8,128)(2,1)S(1)}, bf16[2048,896]{1,0:T(8,128)(2,1)S(1)}, bf16[896,2048]{1,0:T(8,128)(2,1)S(1)}) custom-call(bf16[192,2048]{1,0:T(8,128)(2,1)} %tok.1, bf16[192,2048]{1,0:T(8,128)(2,1)} %cot.1, s32[2,192]{1,0:T(2,128)} %bitcast.12, ...), custom_call_target="tpu_custom_call" | custom-call | tf_op jit(solution)/shard_map/pallas_call | solution.py:553
  63.6 4.3 %shard_map.111 = (bf16[192,256]{1,0:T(8,128)(2,1)}, f32[2,192]{1,0:T(2,128)}, bf16[2048,896]{1,0:T(8,128)(2,1)}, bf16[2048,896]{1,0:T(8,128)(2,1)}, bf16[896,2048]{1,0:T(8,128)(2,1)}) custom-call(bf16[192,256]{1,0:T(8,128)(2,1)S(1)} %get-tuple-element.15.refs_0_, f32[2,192]{1,0:T(2,128)S(1)} %get-tuple-element.16.refs_1_, ...), custom_call_target="tpu_custom_call" | custom-call | tf_op jit(solution)/shard_map/pallas_call | solution.py:611
